TPU v7x, 512 devices: a whole 4x4x16 slice. The times are simulated.
512 devices in a mesh: pp: 16 (over y, x), tp: 32 (over z, core).
Axes of the slice: x: 4, y: 4, z: 16, core: 2. Of those that a mesh axis runs over, the one named last changes fastest.
Arguments:
- entry_stream_rows: bfloat16 [1024, 2048], P('pp', 'tp'), may hold values from -21 to 21
- layer_rescale_factor: float32 [16, 2048], P('pp'), may hold values from 0.1 to 1.9
- probe_projection: bfloat16 [16, 2048, 2048], P('pp', 'tp'), may hold values from -0.125 to 0.125
- retention_projection: bfloat16 [16, 2048, 2048], P('pp', 'tp'), may hold values from -0.125 to 0.125
- candidate_projection: bfloat16 [16, 2048, 2048], P('pp', 'tp'), may hold values from -0.125 to 0.125
- emission_filter_matrix: bfloat16 [16, 2048, 2048], P('pp', 'tp'), may hold values from -0.125 to 0.125
- retention_minimum: float32 [16, 2048], P('pp', 'tp'), may hold values from 0.88 to 0.9921875
- decay_spike: float32 [16, 128, 32], P('pp', None, 'tp'), may hold values from -2.1 to 0
- per_group_scale: float32 [16, 64], P('pp'), may hold values from 0.1 to 1.9
Outputs:
- outputs: bfloat16 [1024, 2048], P('pp', 'tp')
All inputs are finite; a program needn't handle non-finite values.
Results may differ from a plain program's by a relative error of at most 0.03.
Values may be sent and summed in bfloat16 or wider, within the bound.
No kernel may reach another device: no remote copies, remote signals or barrier semaphores. Data moves between devices by JAX's collectives and lax.ppermute only.
A program may use at most 64 MiB of HBM per device.

v0:
```python
import jax
import jax.numpy as jnp
from jax import lax
from jax.sharding import PartitionSpec as P

HEAD = 64
SEG = 64
EPSILON = 1e-06


def shifted(array, axis, by):
    devices = lax.axis_size(axis)
    pairs = [(i, i + by) for i in range(devices) if 0 <= i + by < devices]
    return lax.ppermute(array, axis, pairs)


def from_root(array, axis, root):
    return lax.dynamic_index_in_dim(lax.all_gather(array, axis), root, 0, keepdims=False)


def segment_scan(queries, key_in, log_forget, values, memory):
    head_count = queries.shape[0]
    length = queries.shape[1]
    blocks_count = length // SEG

    def split_blocks(tensor):
        return tensor.reshape(head_count, blocks_count, SEG, tensor.shape[-1]).transpose(1, 0, 2, 3)

    lower_mask = jnp.tril(jnp.ones((SEG, SEG), dtype=bool))[None]

    def one_block(memory_in, pieces):
        block_query, block_key, block_forget, block_value = pieces
        running = jnp.cumsum(block_forget, axis=1)
        query_scaled = block_query * jnp.exp(running)
        key_scaled = block_key * jnp.exp(-running)
        scores = jnp.einsum("hid,hjd->hij", query_scaled, key_scaled)
        scores = jnp.where(lower_mask, scores, 0.0)
        mixed_out = jnp.einsum("hij,hjv->hiv", scores, block_value)
        mixed_out = mixed_out + jnp.einsum("hid,hdv->hiv", query_scaled, memory_in)
        ending = running[:, -1:, :]
        carried_in = jnp.einsum("hjd,hjv->hdv", block_key * jnp.exp(ending - running), block_value)
        memory_out = jnp.exp(ending[:, 0, :])[:, :, None] * memory_in + carried_in
        return (memory_out, mixed_out)

    memory, mixed_out = lax.scan(
        one_block,
        memory,
        (
            split_blocks(queries),
            split_blocks(key_in),
            split_blocks(log_forget),
            split_blocks(values),
        ),
    )
    return (mixed_out.transpose(1, 0, 2, 3).reshape(head_count, length, values.shape[-1]), memory)


def head_norm(mixed_out, channel_gain):
    return (
        mixed_out
        * lax.rsqrt(jnp.mean(mixed_out * mixed_out, axis=-1, keepdims=True) + EPSILON)
        * channel_gain
    )


def shards(
    entry_stream_rows,
    layer_rescale_factor,
    probe_projection,
    retention_projection,
    candidate_projection,
    emission_filter_matrix,
    retention_minimum,
    decay_spike,
    per_group_scale,
):
    sections = lax.axis_size("pp")
    layer_ordinal = lax.axis_index("pp")
    own_rows = entry_stream_rows.shape[0]
    seq_len = 2 * own_rows
    columns = entry_stream_rows.shape[1]
    head_here = columns // HEAD
    model_width = layer_rescale_factor.shape[1]
    micro_count = sections // 2
    per_sequence = seq_len // seq_len
    unit_count = micro_count * per_sequence
    total_steps = unit_count + sections - 1
    entering = lax.all_gather(entry_stream_rows, "pp", axis=0, tiled=True)
    weights = jnp.concatenate(
        [
            probe_projection[0],
            retention_projection[0],
            candidate_projection[0],
            emission_filter_matrix[0],
        ],
        axis=0,
    )
    input_gain = layer_rescale_factor[0]
    lower_edge = retention_minimum[0].reshape(head_here, 1, HEAD)
    spike_collection = decay_spike[0].T
    out_gain = per_group_scale[0]

    def add_piece(piece_in):
        wide_piece = piece_in.astype(jnp.float32)
        scaled = (wide_piece * input_gain[None, :]).astype(jnp.bfloat16)
        product = lax.dot_general(
            scaled, weights, (((1,), (1,)), ((), ())), preferred_element_type=jnp.float32
        )
        return (product, jnp.sum(wide_piece * wide_piece, axis=1))

    def one_step(step_index, carried):
        incoming, memory, finished = carried
        unit_index = step_index - layer_ordinal
        first_slot = jnp.clip(step_index, 0, unit_count - 1)
        fresh_rows = lax.dynamic_slice_in_dim(entering, first_slot * seq_len, seq_len, 0)
        current = jnp.where(layer_ordinal == 0, fresh_rows, incoming)
        projected, squares = add_piece(lax.all_gather(current, "tp", axis=1, tiled=True))
        inverse = lax.rsqrt(squares / model_width + EPSILON)[:, None]
        projected = projected * inverse

        def per_head(role_index):
            picked = projected[:, role_index * columns : (role_index + 1) * columns]
            return picked.reshape(seq_len, head_here, HEAD).transpose(1, 0, 2)

        query_pre = per_head(0)
        forget_pre = per_head(1)
        input_pre = per_head(2)
        gate_pre = per_head(3)
        offset = unit_index % per_sequence * seq_len
        current_surge = spike_collection[:, :, None]
        log_forget = (
            jnp.logaddexp(
                jnp.log(lower_edge), jnp.log1p(-lower_edge) + jax.nn.log_sigmoid(forget_pre)
            )
            + current_surge
        )
        key_in = (1.0 - lower_edge) * jax.nn.sigmoid(-forget_pre)
        queries = jax.nn.silu(query_pre)
        memory = jnp.where(offset == 0, jnp.zeros_like(memory), memory)
        mixed_out, memory = segment_scan(queries, key_in, log_forget, input_pre, memory)
        branch = head_norm(mixed_out, out_gain) * jax.nn.silu(gate_pre)
        branch = branch.transpose(1, 0, 2).reshape(seq_len, columns)
        result = (current.astype(jnp.float32) + branch).astype(jnp.bfloat16)
        passed = shifted(result, "pp", 1)
        out_slot = jnp.clip(unit_index, 0, unit_count - 1)
        write_here = (layer_ordinal == sections - 1) & (unit_index >= 0) & (unit_index < unit_count)
        updated = lax.dynamic_update_slice_in_dim(finished, result, out_slot * seq_len, 0)
        finished = jnp.where(write_here, updated, finished)
        return (passed, memory, finished)

    start_state = (
        jnp.zeros((seq_len, columns), jnp.bfloat16),
        jnp.zeros((head_here, HEAD, HEAD), jnp.float32),
        jnp.zeros((unit_count * seq_len, columns), jnp.bfloat16),
    )
    carried_out = lax.fori_loop(0, total_steps, one_step, start_state)
    everything = from_root(carried_out[2], "pp", sections - 1)
    return lax.dynamic_slice_in_dim(everything, layer_ordinal * own_rows, own_rows, 0)


def solution(mesh):
    in_specs = (
        P("pp", "tp"),
        P("pp", None),
        P("pp", "tp", None),
        P("pp", "tp", None),
        P("pp", "tp", None),
        P("pp", "tp", None),
        P("pp", "tp"),
        P("pp", None, "tp"),
        P("pp", None),
    )
    out_specs = P("pp", "tp")
    return jax.shard_map(shards, mesh=mesh, in_specs=in_specs, out_specs=out_specs, check_vma=False)
```

profile of v0, /device:TPU:1, one launch (start us, length us, event | category | flops | bytes accessed | tf_op | source)
XLA Modules:
  0.0 1040.1 jit_solution(864880211558230233)
XLA Ops:
  28.3 930.2 %while.59 = (s32[]{:T(128)}, bf16[128,64]{1,0:T(8,128)(2,1)S(1)}, bf16[1024,64]{1,0:T(8,128)(2,1)S(1)}, pred[]{:T(512)}, bf16[1024,64]{1,0:T(8,128)(2,1)S(1)}, /...) while((s32[]{:T(128)}, bf16[128,64]{1,0:T(8,128)(2,1)S(1)}, ...), condition=%wide.region_6.7_spmd, body=%wide.region_0.6_spmd.sunk | while | flops 138551632 | bytes 3955077 | solution.py:156
  28.5 43.4 %all_gather.24 = bf16[128,2048]{0,1:T(8,128)(2,1)S(1)} all-gather(bf16[128,64]{0,1:T(8,128)(2,1)S(1)} %copy.20), channel_id=1, replica_groups=mesh['pp'=16,'tp'=32] {'tp'}, dimensions={1}, use_global_device_ids=true | all-gather | bytes 540672 | tf_op jit(solution)/shard_map/while/body/eval_jaxpr/all_gather | solution.py:117
  79.0 29.1 %all_gather.24 = bf16[128,2048]{0,1:T(8,128)(2,1)S(1)} all-gather(bf16[128,64]{0,1:T(8,128)(2,1)S(1)} %copy.20), channel_id=1, replica_groups=mesh['pp'=16,'tp'=32] {'tp'}, dimensions={1}, use_global_device_ids=true | all-gather | bytes 540672 | tf_op jit(solution)/shard_map/while/body/eval_jaxpr/all_gather | solution.py:117
  116.3 31.0 %all_gather.24 = bf16[128,2048]{0,1:T(8,128)(2,1)S(1)} all-gather(bf16[128,64]{0,1:T(8,128)(2,1)S(1)} %copy.20), channel_id=1, replica_groups=mesh['pp'=16,'tp'=32] {'tp'}, dimensions={1}, use_global_device_ids=true | all-gather | bytes 540672 | tf_op jit(solution)/shard_map/while/body/eval_jaxpr/all_gather | solution.py:117
  192.9 31.0 %all_gather.24 = bf16[128,2048]{0,1:T(8,128)(2,1)S(1)} all-gather(bf16[128,64]{0,1:T(8,128)(2,1)S(1)} %copy.20), channel_id=1, replica_groups=mesh['pp'=16,'tp'=32] {'tp'}, dimensions={1}, use_global_device_ids=true | all-gather | bytes 540672 | tf_op jit(solution)/shard_map/while/body/eval_jaxpr/all_gather | solution.py:117
  232.2 29.1 %all_gather.24 = bf16[128,2048]{0,1:T(8,128)(2,1)S(1)} all-gather(bf16[128,64]{0,1:T(8,128)(2,1)S(1)} %copy.20), channel_id=1, replica_groups=mesh['pp'=16,'tp'=32] {'tp'}, dimensions={1}, use_global_device_ids=true | all-gather | bytes 540672 | tf_op jit(solution)/shard_map/while/body/eval_jaxpr/all_gather | solution.py:117
  270.9 31.0 %all_gather.24 = bf16[128,2048]{0,1:T(8,128)(2,1)S(1)} all-gather(bf16[128,64]{0,1:T(8,128)(2,1)S(1)} %copy.20), channel_id=1, replica_groups=mesh['pp'=16,'tp'=32] {'tp'}, dimensions={1}, use_global_device_ids=true | all-gather | bytes 540672 | tf_op jit(solution)/shard_map/while/body/eval_jaxpr/all_gather | solution.py:117
  312.2 29.1 %all_gather.24 = bf16[128,2048]{0,1:T(8,128)(2,1)S(1)} all-gather(bf16[128,64]{0,1:T(8,128)(2,1)S(1)} %copy.20), channel_id=1, replica_groups=mesh['pp'=16,'tp'=32] {'tp'}, dimensions={1}, use_global_device_ids=true | all-gather | bytes 540672 | tf_op jit(solution)/shard_map/while/body/eval_jaxpr/all_gather | solution.py:117
  351.7 31.0 %all_gather.24 = bf16[128,2048]{0,1:T(8,128)(2,1)S(1)} all-gather(bf16[128,64]{0,1:T(8,128)(2,1)S(1)} %copy.20), channel_id=1, replica_groups=mesh['pp'=16,'tp'=32] {'tp'}, dimensions={1}, use_global_device_ids=true | all-gather | bytes 540672 | tf_op jit(solution)/shard_map/while/body/eval_jaxpr/all_gather | solution.py:117
  393.0 29.1 %all_gather.24 = bf16[128,2048]{0,1:T(8,128)(2,1)S(1)} all-gather(bf16[128,64]{0,1:T(8,128)(2,1)S(1)} %copy.20), channel_id=1, replica_groups=mesh['pp'=16,'tp'=32] {'tp'}, dimensions={1}, use_global_device_ids=true | all-gather | bytes 540672 | tf_op jit(solution)/shard_map/while/body/eval_jaxpr/all_gather | solution.py:117
  432.5 31.0 %all_gather.24 = bf16[128,2048]{0,1:T(8,128)(2,1)S(1)} all-gather(bf16[128,64]{0,1:T(8,128)(2,1)S(1)} %copy.20), channel_id=1, replica_groups=mesh['pp'=16,'tp'=32] {'tp'}, dimensions={1}, use_global_device_ids=true | all-gather | bytes 540672 | tf_op jit(solution)/shard_map/while/body/eval_jaxpr/all_gather | solution.py:117
  473.8 29.1 %all_gather.24 = bf16[128,2048]{0,1:T(8,128)(2,1)S(1)} all-gather(bf16[128,64]{0,1:T(8,128)(2,1)S(1)} %copy.20), channel_id=1, replica_groups=mesh['pp'=16,'tp'=32] {'tp'}, dimensions={1}, use_global_device_ids=true | all-gather | bytes 540672 | tf_op jit(solution)/shard_map/while/body/eval_jaxpr/all_gather | solution.py:117
  513.3 31.0 %all_gather.24 = bf16[128,2048]{0,1:T(8,128)(2,1)S(1)} all-gather(bf16[128,64]{0,1:T(8,128)(2,1)S(1)} %copy.20), channel_id=1, replica_groups=mesh['pp'=16,'tp'=32] {'tp'}, dimensions={1}, use_global_device_ids=true | all-gather | bytes 540672 | tf_op jit(solution)/shard_map/while/body/eval_jaxpr/all_gather | solution.py:117
  554.6 29.1 %all_gather.24 = bf16[128,2048]{0,1:T(8,128)(2,1)S(1)} all-gather(bf16[128,64]{0,1:T(8,128)(2,1)S(1)} %copy.20), channel_id=1, replica_groups=mesh['pp'=16,'tp'=32] {'tp'}, dimensions={1}, use_global_device_ids=true | all-gather | bytes 540672 | tf_op jit(solution)/shard_map/while/body/eval_jaxpr/all_gather | solution.py:117
  594.1 31.0 %all_gather.24 = bf16[128,2048]{0,1:T(8,128)(2,1)S(1)} all-gather(bf16[128,64]{0,1:T(8,128)(2,1)S(1)} %copy.20), channel_id=1, replica_groups=mesh['pp'=16,'tp'=32] {'tp'}, dimensions={1}, use_global_device_ids=true | all-gather | bytes 540672 | tf_op jit(solution)/shard_map/while/body/eval_jaxpr/all_gather | solution.py:117
  635.4 29.1 %all_gather.24 = bf16[128,2048]{0,1:T(8,128)(2,1)S(1)} all-gather(bf16[128,64]{0,1:T(8,128)(2,1)S(1)} %copy.20), channel_id=1, replica_groups=mesh['pp'=16,'tp'=32] {'tp'}, dimensions={1}, use_global_device_ids=true | all-gather | bytes 540672 | tf_op jit(solution)/shard_map/while/body/eval_jaxpr/all_gather | solution.py:117
  674.9 31.0 %all_gather.24 = bf16[128,2048]{0,1:T(8,128)(2,1)S(1)} all-gather(bf16[128,64]{0,1:T(8,128)(2,1)S(1)} %copy.20), channel_id=1, replica_groups=mesh['pp'=16,'tp'=32] {'tp'}, dimensions={1}, use_global_device_ids=true | all-gather | bytes 540672 | tf_op jit(solution)/shard_map/while/body/eval_jaxpr/all_gather | solution.py:117
  716.2 29.1 %all_gather.24 = bf16[128,2048]{0,1:T(8,128)(2,1)S(1)} all-gather(bf16[128,64]{0,1:T(8,128)(2,1)S(1)} %copy.20), channel_id=1, replica_groups=mesh['pp'=16,'tp'=32] {'tp'}, dimensions={1}, use_global_device_ids=true | all-gather | bytes 540672 | tf_op jit(solution)/shard_map/while/body/eval_jaxpr/all_gather | solution.py:117
  755.7 31.0 %all_gather.24 = bf16[128,2048]{0,1:T(8,128)(2,1)S(1)} all-gather(bf16[128,64]{0,1:T(8,128)(2,1)S(1)} %copy.20), channel_id=1, replica_groups=mesh['pp'=16,'tp'=32] {'tp'}, dimensions={1}, use_global_device_ids=true | all-gather | bytes 540672 | tf_op jit(solution)/shard_map/while/body/eval_jaxpr/all_gather | solution.py:117
  797.0 29.1 %all_gather.24 = bf16[128,2048]{0,1:T(8,128)(2,1)S(1)} all-gather(bf16[128,64]{0,1:T(8,128)(2,1)S(1)} %copy.20), channel_id=1, replica_groups=mesh['pp'=16,'tp'=32] {'tp'}, dimensions={1}, use_global_device_ids=true | all-gather | bytes 540672 | tf_op jit(solution)/shard_map/while/body/eval_jaxpr/all_gather | solution.py:117
  836.5 31.0 %all_gather.24 = bf16[128,2048]{0,1:T(8,128)(2,1)S(1)} all-gather(bf16[128,64]{0,1:T(8,128)(2,1)S(1)} %copy.20), channel_id=1, replica_groups=mesh['pp'=16,'tp'=32] {'tp'}, dimensions={1}, use_global_device_ids=true | all-gather | bytes 540672 | tf_op jit(solution)/shard_map/while/body/eval_jaxpr/all_gather | solution.py:117
  877.8 29.1 %all_gather.24 = bf16[128,2048]{0,1:T(8,128)(2,1)S(1)} all-gather(bf16[128,64]{0,1:T(8,128)(2,1)S(1)} %copy.20), channel_id=1, replica_groups=mesh['pp'=16,'tp'=32] {'tp'}, dimensions={1}, use_global_device_ids=true | all-gather | bytes 540672 | tf_op jit(solution)/shard_map/while/body/eval_jaxpr/all_gather | solution.py:117
  917.3 31.0 %all_gather.24 = bf16[128,2048]{0,1:T(8,128)(2,1)S(1)} all-gather(bf16[128,64]{0,1:T(8,128)(2,1)S(1)} %copy.20), channel_id=1, replica_groups=mesh['pp'=16,'tp'=32] {'tp'}, dimensions={1}, use_global_device_ids=true | all-gather | bytes 540672 | tf_op jit(solution)/shard_map/while/body/eval_jaxpr/all_gather | solution.py:117
  959.3 72.4 %all-gather.3.cloned.1.call-done = bf16[16384,64]{1,0:T(8,128)(2,1)} async-done(((bf16[1024,64]{1,0:T(8,128)(2,1)}), bf16[16384,64]{1,0:T(8,128)(2,1)}) %all-gather.3.cloned.1.call-update) | async-done | bytes 2097168 | tf_op jit(solution)/shard_map/all_gather | solution.py:18
  (733 shorter events, 309.2 us)
Async XLA Ops:
  6.5 1025.1 %all-gather.3.cloned.1.call-start = ((), (), s32[]{:S(2)}) async-start(), calls=%async_computation | async-start | bytes 4456448 | tf_op jit(solution)/shard_map/all_gather | solution.py:18
  75.0 3.8 collective-permute-start
  111.2 5.0 collective-permute-start
  150.5 5.0 collective-permute-start
  187.8 5.0 collective-permute-start
  227.1 5.0 collective-permute-start
  264.4 6.3 collective-permute-start
  305.0 7.1 collective-permute-start
  344.5 7.1 collective-permute-start
  385.8 7.1 collective-permute-start
  425.3 7.1 collective-permute-start
  466.7 7.1 collective-permute-start
  506.1 7.1 collective-permute-start
  547.5 7.1 collective-permute-start
  586.9 7.1 collective-permute-start
  628.3 7.1 collective-permute-start
  667.7 7.1 collective-permute-start
  709.1 7.1 collective-permute-start
  748.5 7.1 collective-permute-start
  789.9 7.1 collective-permute-start
  829.3 7.1 collective-permute-start
  870.7 7.1 collective-permute-start
  910.1 7.1 collective-permute-start
  951.5 7.1 collective-permute-start
  (5 other events, 87.6 us)
Sparse Core Ops, SparseCore 0:
  959.4 72.2 all-gather.2
where the time goes:
time: 1040 us
  blocking collectives  724 us (70%)
  starting transfers between devices  127 us (12%)
  waiting for transfers between devices  95.4 us (9%)
  matrix products  47.4 us (5%)
  other arithmetic  23.2 us (2%)
  between operations  13.5 us (1%)
    all_gather x23, blocking collectives, one_step(): lax.all_gather(current, 'tp', axis=1, tiled=True)  704 us
    ppermute x23, starting transfers between devices, shifted(): return lax.ppermute(array, axis, pairs)  127 us
    all_gather x1, waiting for transfers between devices, from_root(): lax.all_gather(array, axis)  72.4 us
    ppermute x23, waiting for transfers between devices, shifted(): return lax.ppermute(array, axis, pairs)  23 us
  transfers between devices with their start and end apart: 24, of which 24 were waited for; matrix products, arithmetic and copies ran while one was open for 0% of the time, Pallas kernels for 0%

commit v1 on v0

--- a/solution.py
+++ b/solution.py
@@ -114,7 +114,11 @@
         first_slot = jnp.clip(step_index, 0, unit_count - 1)
         fresh_rows = lax.dynamic_slice_in_dim(entering, first_slot * seq_len, seq_len, 0)
         current = jnp.where(layer_ordinal == 0, fresh_rows, incoming)
-        projected, squares = add_piece(lax.all_gather(current, "tp", axis=1, tiled=True))
+        projected, squares = add_piece(
+            jnp.concatenate(
+                lax.all_to_all(jnp.stack([current] * lax.axis_size("tp")), "tp", 0, 0), axis=1
+            )
+        )
         inverse = lax.rsqrt(squares / model_width + EPSILON)[:, None]
         projected = projected * inverse
 

time: 1040 us -> 1260 us (1.21)
  waiting for transfers between devices: 95.4 us -> 861 us
  blocking collectives: 724 us -> 19.7 us
  starting transfers between devices: 127 us -> 262 us
  local copies, waits for them, and re-layouts: 7.26 us -> 28.5 us
    all_to_all x0 -> x23, waiting for transfers between devices: none -> 770 us  [one_step(): lax.all_to_all(jnp.stack([current] * lax.axis_size('tp')), 'tp', 0, 0)]
    all_gather x23 -> x0, blocking collectives: 704 us -> none  [one_step(): lax.all_gather(current, 'tp', axis=1, tiled=True)]
    all_to_all x0 -> x23, starting transfers between devices: none -> 135 us  [one_step(): lax.all_to_all(jnp.stack([current] * lax.axis_size('tp')), 'tp', 0, 0)]
    another operation x0 -> x23, local copies, waits for them, and re-layouts: none -> 21.2 us  [one_step(): jnp.stack([current] * lax.axis_size('tp'))]
  transfers between devices with their start and end apart: 24 -> 47, of which waited for: 24 -> 47; matrix products, arithmetic and copies ran while one was open for 0% -> 0% of each run, Pallas kernels for 0% -> 0%
where the time goes in v1:
time: 1260 us
  waiting for transfers between devices  861 us (68%)
  starting transfers between devices  262 us (21%)
  matrix products  37.8 us (3%)
  other arithmetic  31.1 us (2%)
  local copies, waits for them, and re-layouts  28.5 us (2%)
  blocking collectives  19.7 us (2%)
  between operations  13.5 us (1%)
    all_to_all x23, waiting for transfers between devices, one_step(): lax.all_to_all(jnp.stack([current] * lax.axis_size('tp')), 'tp', 0, 0)  770 us
    all_to_all x23, starting transfers between devices, one_step(): lax.all_to_all(jnp.stack([current] * lax.axis_size('tp')), 'tp', 0, 0)  135 us
    ppermute x23, starting transfers between devices, shifted(): return lax.ppermute(array, axis, pairs)  127 us
    all_gather x1, waiting for transfers between devices, from_root(): lax.all_gather(array, axis)  68.2 us
  transfers between devices with their start and end apart: 47, of which 47 were waited for; matrix products, arithmetic and copies ran while one was open for 0% of the time, Pallas kernels for 0%

profile of v1, /device:TPU:1, one launch (start us, length us, event | category | flops | bytes accessed | tf_op | source)
XLA Modules:
  0.0 1257.2 jit_solution(15405859471785468717)
XLA Ops:
  28.3 1151.4 %while.59 = (s32[]{:T(128)}, bf16[128,64]{1,0:T(8,128)(2,1)S(1)}, bf16[1024,64]{1,0:T(8,128)(2,1)S(1)}, pred[]{:T(512)}, bf16[1024,64]{1,0:T(8,128)(2,1)S(1)}, /...) while((s32[]{:T(128)}, bf16[128,64]{1,0:T(8,128)(2,1)S(1)}, ...), condition=%wide.region_6.7_spmd, body=%wide.region_0.6_spmd.sunk | while | flops 138551632 | bytes 6576549 | solution.py:160
  97.0 33.5 %all-to-all-done = bf16[32,128,64]{1,2,0:T(8,128)(2,1)S(1)} async-done(((bf16[32,128,64]{1,2,0:T(8,128)(2,1)}), bf16[32,128,64]{1,2,0:T(8,128)(2,1)S(1)}, u32[]{:S(2)}, u32[]{:S(2)}) %all-to-all-start) | async-done | bytes 524320 | tf_op jit(solution)/shard_map/while/body/eval_jaxpr/all_to_all | solution.py:119
  144.8 33.5 %all-to-all-done = bf16[32,128,64]{1,2,0:T(8,128)(2,1)S(1)} async-done(((bf16[32,128,64]{1,2,0:T(8,128)(2,1)}), bf16[32,128,64]{1,2,0:T(8,128)(2,1)S(1)}, u32[]{:S(2)}, u32[]{:S(2)}) %all-to-all-start) | async-done | bytes 524320 | tf_op jit(solution)/shard_map/while/body/eval_jaxpr/all_to_all | solution.py:119
  192.6 33.5 %all-to-all-done = bf16[32,128,64]{1,2,0:T(8,128)(2,1)S(1)} async-done(((bf16[32,128,64]{1,2,0:T(8,128)(2,1)}), bf16[32,128,64]{1,2,0:T(8,128)(2,1)S(1)}, u32[]{:S(2)}, u32[]{:S(2)}) %all-to-all-start) | async-done | bytes 524320 | tf_op jit(solution)/shard_map/while/body/eval_jaxpr/all_to_all | solution.py:119
  240.4 33.5 %all-to-all-done = bf16[32,128,64]{1,2,0:T(8,128)(2,1)S(1)} async-done(((bf16[32,128,64]{1,2,0:T(8,128)(2,1)}), bf16[32,128,64]{1,2,0:T(8,128)(2,1)S(1)}, u32[]{:S(2)}, u32[]{:S(2)}) %all-to-all-start) | async-done | bytes 524320 | tf_op jit(solution)/shard_map/while/body/eval_jaxpr/all_to_all | solution.py:119
  288.2 33.5 %all-to-all-done = bf16[32,128,64]{1,2,0:T(8,128)(2,1)S(1)} async-done(((bf16[32,128,64]{1,2,0:T(8,128)(2,1)}), bf16[32,128,64]{1,2,0:T(8,128)(2,1)S(1)}, u32[]{:S(2)}, u32[]{:S(2)}) %all-to-all-start) | async-done | bytes 524320 | tf_op jit(solution)/shard_map/while/body/eval_jaxpr/all_to_all | solution.py:119
  337.4 33.5 %all-to-all-done = bf16[32,128,64]{1,2,0:T(8,128)(2,1)S(1)} async-done(((bf16[32,128,64]{1,2,0:T(8,128)(2,1)}), bf16[32,128,64]{1,2,0:T(8,128)(2,1)S(1)}, u32[]{:S(2)}, u32[]{:S(2)}) %all-to-all-start) | async-done | bytes 524320 | tf_op jit(solution)/shard_map/while/body/eval_jaxpr/all_to_all | solution.py:119
  387.3 33.5 %all-to-all-done = bf16[32,128,64]{1,2,0:T(8,128)(2,1)S(1)} async-done(((bf16[32,128,64]{1,2,0:T(8,128)(2,1)}), bf16[32,128,64]{1,2,0:T(8,128)(2,1)S(1)}, u32[]{:S(2)}, u32[]{:S(2)}) %all-to-all-start) | async-done | bytes 524320 | tf_op jit(solution)/shard_map/while/body/eval_jaxpr/all_to_all | solution.py:119
  437.2 33.5 %all-to-all-done = bf16[32,128,64]{1,2,0:T(8,128)(2,1)S(1)} async-done(((bf16[32,128,64]{1,2,0:T(8,128)(2,1)}), bf16[32,128,64]{1,2,0:T(8,128)(2,1)S(1)}, u32[]{:S(2)}, u32[]{:S(2)}) %all-to-all-start) | async-done | bytes 524320 | tf_op jit(solution)/shard_map/while/body/eval_jaxpr/all_to_all | solution.py:119
  487.2 33.5 %all-to-all-done = bf16[32,128,64]{1,2,0:T(8,128)(2,1)S(1)} async-done(((bf16[32,128,64]{1,2,0:T(8,128)(2,1)}), bf16[32,128,64]{1,2,0:T(8,128)(2,1)S(1)}, u32[]{:S(2)}, u32[]{:S(2)}) %all-to-all-start) | async-done | bytes 524320 | tf_op jit(solution)/shard_map/while/body/eval_jaxpr/all_to_all | solution.py:119
  537.1 33.5 %all-to-all-done = bf16[32,128,64]{1,2,0:T(8,128)(2,1)S(1)} async-done(((bf16[32,128,64]{1,2,0:T(8,128)(2,1)}), bf16[32,128,64]{1,2,0:T(8,128)(2,1)S(1)}, u32[]{:S(2)}, u32[]{:S(2)}) %all-to-all-start) | async-done | bytes 524320 | tf_op jit(solution)/shard_map/while/body/eval_jaxpr/all_to_all | solution.py:119
  587.0 33.5 %all-to-all-done = bf16[32,128,64]{1,2,0:T(8,128)(2,1)S(1)} async-done(((bf16[32,128,64]{1,2,0:T(8,128)(2,1)}), bf16[32,128,64]{1,2,0:T(8,128)(2,1)S(1)}, u32[]{:S(2)}, u32[]{:S(2)}) %all-to-all-start) | async-done | bytes 524320 | tf_op jit(solution)/shard_map/while/body/eval_jaxpr/all_to_all | solution.py:119
  636.9 33.5 %all-to-all-done = bf16[32,128,64]{1,2,0:T(8,128)(2,1)S(1)} async-done(((bf16[32,128,64]{1,2,0:T(8,128)(2,1)}), bf16[32,128,64]{1,2,0:T(8,128)(2,1)S(1)}, u32[]{:S(2)}, u32[]{:S(2)}) %all-to-all-start) | async-done | bytes 524320 | tf_op jit(solution)/shard_map/while/body/eval_jaxpr/all_to_all | solution.py:119
  686.8 33.5 %all-to-all-done = bf16[32,128,64]{1,2,0:T(8,128)(2,1)S(1)} async-done(((bf16[32,128,64]{1,2,0:T(8,128)(2,1)}), bf16[32,128,64]{1,2,0:T(8,128)(2,1)S(1)}, u32[]{:S(2)}, u32[]{:S(2)}) %all-to-all-start) | async-done | bytes 524320 | tf_op jit(solution)/shard_map/while/body/eval_jaxpr/all_to_all | solution.py:119
  736.8 33.5 %all-to-all-done = bf16[32,128,64]{1,2,0:T(8,128)(2,1)S(1)} async-done(((bf16[32,128,64]{1,2,0:T(8,128)(2,1)}), bf16[32,128,64]{1,2,0:T(8,128)(2,1)S(1)}, u32[]{:S(2)}, u32[]{:S(2)}) %all-to-all-start) | async-done | bytes 524320 | tf_op jit(solution)/shard_map/while/body/eval_jaxpr/all_to_all | solution.py:119
  786.7 33.5 %all-to-all-done = bf16[32,128,64]{1,2,0:T(8,128)(2,1)S(1)} async-done(((bf16[32,128,64]{1,2,0:T(8,128)(2,1)}), bf16[32,128,64]{1,2,0:T(8,128)(2,1)S(1)}, u32[]{:S(2)}, u32[]{:S(2)}) %all-to-all-start) | async-done | bytes 524320 | tf_op jit(solution)/shard_map/while/body/eval_jaxpr/all_to_all | solution.py:119
  836.6 33.5 %all-to-all-done = bf16[32,128,64]{1,2,0:T(8,128)(2,1)S(1)} async-done(((bf16[32,128,64]{1,2,0:T(8,128)(2,1)}), bf16[32,128,64]{1,2,0:T(8,128)(2,1)S(1)}, u32[]{:S(2)}, u32[]{:S(2)}) %all-to-all-start) | async-done | bytes 524320 | tf_op jit(solution)/shard_map/while/body/eval_jaxpr/all_to_all | solution.py:119
  886.5 33.5 %all-to-all-done = bf16[32,128,64]{1,2,0:T(8,128)(2,1)S(1)} async-done(((bf16[32,128,64]{1,2,0:T(8,128)(2,1)}), bf16[32,128,64]{1,2,0:T(8,128)(2,1)S(1)}, u32[]{:S(2)}, u32[]{:S(2)}) %all-to-all-start) | async-done | bytes 524320 | tf_op jit(solution)/shard_map/while/body/eval_jaxpr/all_to_all | solution.py:119
  936.4 33.5 %all-to-all-done = bf16[32,128,64]{1,2,0:T(8,128)(2,1)S(1)} async-done(((bf16[32,128,64]{1,2,0:T(8,128)(2,1)}), bf16[32,128,64]{1,2,0:T(8,128)(2,1)S(1)}, u32[]{:S(2)}, u32[]{:S(2)}) %all-to-all-start) | async-done | bytes 524320 | tf_op jit(solution)/shard_map/while/body/eval_jaxpr/all_to_all | solution.py:119
  986.4 33.5 %all-to-all-done = bf16[32,128,64]{1,2,0:T(8,128)(2,1)S(1)} async-done(((bf16[32,128,64]{1,2,0:T(8,128)(2,1)}), bf16[32,128,64]{1,2,0:T(8,128)(2,1)S(1)}, u32[]{:S(2)}, u32[]{:S(2)}) %all-to-all-start) | async-done | bytes 524320 | tf_op jit(solution)/shard_map/while/body/eval_jaxpr/all_to_all | solution.py:119
  1036.3 33.5 %all-to-all-done = bf16[32,128,64]{1,2,0:T(8,128)(2,1)S(1)} async-done(((bf16[32,128,64]{1,2,0:T(8,128)(2,1)}), bf16[32,128,64]{1,2,0:T(8,128)(2,1)S(1)}, u32[]{:S(2)}, u32[]{:S(2)}) %all-to-all-start) | async-done | bytes 524320 | tf_op jit(solution)/shard_map/while/body/eval_jaxpr/all_to_all | solution.py:119
  1086.2 33.5 %all-to-all-done = bf16[32,128,64]{1,2,0:T(8,128)(2,1)S(1)} async-done(((bf16[32,128,64]{1,2,0:T(8,128)(2,1)}), bf16[32,128,64]{1,2,0:T(8,128)(2,1)S(1)}, u32[]{:S(2)}, u32[]{:S(2)}) %all-to-all-start) | async-done | bytes 524320 | tf_op jit(solution)/shard_map/while/body/eval_jaxpr/all_to_all | solution.py:119
  1136.1 33.5 %all-to-all-done = bf16[32,128,64]{1,2,0:T(8,128)(2,1)S(1)} async-done(((bf16[32,128,64]{1,2,0:T(8,128)(2,1)}), bf16[32,128,64]{1,2,0:T(8,128)(2,1)S(1)}, u32[]{:S(2)}, u32[]{:S(2)}) %all-to-all-start) | async-done | bytes 524320 | tf_op jit(solution)/shard_map/while/body/eval_jaxpr/all_to_all | solution.py:119
  1180.5 68.2 %all-gather.3.cloned.1.call-done = bf16[16384,64]{1,0:T(8,128)(2,1)} async-done(((bf16[1024,64]{1,0:T(8,128)(2,1)}), bf16[16384,64]{1,0:T(8,128)(2,1)}) %all-gather.3.cloned.1.call-update) | async-done | bytes 2097168 | tf_op jit(solution)/shard_map/all_gather | solution.py:18
  (802 shorter events, 468.1 us)
Async XLA Ops:
  6.5 1242.2 %all-gather.3.cloned.1.call-start = ((), (), s32[]{:S(2)}) async-start(), calls=%async_computation.1 | async-start | bytes 4456448 | tf_op jit(solution)/shard_map/all_gather | solution.py:18
  29.4 54.7 %all-to-all-start = ((bf16[32,128,64]{1,2,0:T(8,128)(2,1)}), bf16[32,128,64]{1,2,0:T(8,128)(2,1)S(1)}, u32[]{:S(2)}, u32[]{:S(2)}) async-start(bf16[32,128,64]{1,2,0:T(8,128)(2,1)} %stack.7), calls=%async_computation | async-start | bytes 1048576 | tf_op jit(solution)/shard_map/while/body/eval_jaxpr/all_to_all | solution.py:119
  92.0 38.4 %all-to-all-start = ((bf16[32,128,64]{1,2,0:T(8,128)(2,1)}), bf16[32,128,64]{1,2,0:T(8,128)(2,1)S(1)}, u32[]{:S(2)}, u32[]{:S(2)}) async-start(bf16[32,128,64]{1,2,0:T(8,128)(2,1)} %stack.7), calls=%async_computation | async-start | bytes 1048576 | tf_op jit(solution)/shard_map/while/body/eval_jaxpr/all_to_all | solution.py:119
  139.5 38.7 %all-to-all-start = ((bf16[32,128,64]{1,2,0:T(8,128)(2,1)}), bf16[32,128,64]{1,2,0:T(8,128)(2,1)S(1)}, u32[]{:S(2)}, u32[]{:S(2)}) async-start(bf16[32,128,64]{1,2,0:T(8,128)(2,1)} %stack.7), calls=%async_computation | async-start | bytes 1048576 | tf_op jit(solution)/shard_map/while/body/eval_jaxpr/all_to_all | solution.py:119
  187.3 38.7 %all-to-all-start = ((bf16[32,128,64]{1,2,0:T(8,128)(2,1)}), bf16[32,128,64]{1,2,0:T(8,128)(2,1)S(1)}, u32[]{:S(2)}, u32[]{:S(2)}) async-start(bf16[32,128,64]{1,2,0:T(8,128)(2,1)} %stack.7), calls=%async_computation | async-start | bytes 1048576 | tf_op jit(solution)/shard_map/while/body/eval_jaxpr/all_to_all | solution.py:119
  235.2 38.7 %all-to-all-start = ((bf16[32,128,64]{1,2,0:T(8,128)(2,1)}), bf16[32,128,64]{1,2,0:T(8,128)(2,1)S(1)}, u32[]{:S(2)}, u32[]{:S(2)}) async-start(bf16[32,128,64]{1,2,0:T(8,128)(2,1)} %stack.7), calls=%async_computation | async-start | bytes 1048576 | tf_op jit(solution)/shard_map/while/body/eval_jaxpr/all_to_all | solution.py:119
  283.0 38.7 %all-to-all-start = ((bf16[32,128,64]{1,2,0:T(8,128)(2,1)}), bf16[32,128,64]{1,2,0:T(8,128)(2,1)S(1)}, u32[]{:S(2)}, u32[]{:S(2)}) async-start(bf16[32,128,64]{1,2,0:T(8,128)(2,1)} %stack.7), calls=%async_computation | async-start | bytes 1048576 | tf_op jit(solution)/shard_map/while/body/eval_jaxpr/all_to_all | solution.py:119
  332.1 38.7 %all-to-all-start = ((bf16[32,128,64]{1,2,0:T(8,128)(2,1)}), bf16[32,128,64]{1,2,0:T(8,128)(2,1)S(1)}, u32[]{:S(2)}, u32[]{:S(2)}) async-start(bf16[32,128,64]{1,2,0:T(8,128)(2,1)} %stack.7), calls=%async_computation | async-start | bytes 1048576 | tf_op jit(solution)/shard_map/while/body/eval_jaxpr/all_to_all | solution.py:119
  382.1 38.7 %all-to-all-start = ((bf16[32,128,64]{1,2,0:T(8,128)(2,1)}), bf16[32,128,64]{1,2,0:T(8,128)(2,1)S(1)}, u32[]{:S(2)}, u32[]{:S(2)}) async-start(bf16[32,128,64]{1,2,0:T(8,128)(2,1)} %stack.7), calls=%async_computation | async-start | bytes 1048576 | tf_op jit(solution)/shard_map/while/body/eval_jaxpr/all_to_all | solution.py:119
  432.0 38.7 %all-to-all-start = ((bf16[32,128,64]{1,2,0:T(8,128)(2,1)}), bf16[32,128,64]{1,2,0:T(8,128)(2,1)S(1)}, u32[]{:S(2)}, u32[]{:S(2)}) async-start(bf16[32,128,64]{1,2,0:T(8,128)(2,1)} %stack.7), calls=%async_computation | async-start | bytes 1048576 | tf_op jit(solution)/shard_map/while/body/eval_jaxpr/all_to_all | solution.py:119
  481.9 38.7 %all-to-all-start = ((bf16[32,128,64]{1,2,0:T(8,128)(2,1)}), bf16[32,128,64]{1,2,0:T(8,128)(2,1)S(1)}, u32[]{:S(2)}, u32[]{:S(2)}) async-start(bf16[32,128,64]{1,2,0:T(8,128)(2,1)} %stack.7), calls=%async_computation | async-start | bytes 1048576 | tf_op jit(solution)/shard_map/while/body/eval_jaxpr/all_to_all | solution.py:119
  531.8 38.7 %all-to-all-start = ((bf16[32,128,64]{1,2,0:T(8,128)(2,1)}), bf16[32,128,64]{1,2,0:T(8,128)(2,1)S(1)}, u32[]{:S(2)}, u32[]{:S(2)}) async-start(bf16[32,128,64]{1,2,0:T(8,128)(2,1)} %stack.7), calls=%async_computation | async-start | bytes 1048576 | tf_op jit(solution)/shard_map/while/body/eval_jaxpr/all_to_all | solution.py:119
  581.7 38.7 %all-to-all-start = ((bf16[32,128,64]{1,2,0:T(8,128)(2,1)}), bf16[32,128,64]{1,2,0:T(8,128)(2,1)S(1)}, u32[]{:S(2)}, u32[]{:S(2)}) async-start(bf16[32,128,64]{1,2,0:T(8,128)(2,1)} %stack.7), calls=%async_computation | async-start | bytes 1048576 | tf_op jit(solution)/shard_map/while/body/eval_jaxpr/all_to_all | solution.py:119
  631.7 38.7 %all-to-all-start = ((bf16[32,128,64]{1,2,0:T(8,128)(2,1)}), bf16[32,128,64]{1,2,0:T(8,128)(2,1)S(1)}, u32[]{:S(2)}, u32[]{:S(2)}) async-start(bf16[32,128,64]{1,2,0:T(8,128)(2,1)} %stack.7), calls=%async_computation | async-start | bytes 1048576 | tf_op jit(solution)/shard_map/while/body/eval_jaxpr/all_to_all | solution.py:119
  681.6 38.7 %all-to-all-start = ((bf16[32,128,64]{1,2,0:T(8,128)(2,1)}), bf16[32,128,64]{1,2,0:T(8,128)(2,1)S(1)}, u32[]{:S(2)}, u32[]{:S(2)}) async-start(bf16[32,128,64]{1,2,0:T(8,128)(2,1)} %stack.7), calls=%async_computation | async-start | bytes 1048576 | tf_op jit(solution)/shard_map/while/body/eval_jaxpr/all_to_all | solution.py:119
  731.5 38.7 %all-to-all-start = ((bf16[32,128,64]{1,2,0:T(8,128)(2,1)}), bf16[32,128,64]{1,2,0:T(8,128)(2,1)S(1)}, u32[]{:S(2)}, u32[]{:S(2)}) async-start(bf16[32,128,64]{1,2,0:T(8,128)(2,1)} %stack.7), calls=%async_computation | async-start | bytes 1048576 | tf_op jit(solution)/shard_map/while/body/eval_jaxpr/all_to_all | solution.py:119
  781.4 38.7 %all-to-all-start = ((bf16[32,128,64]{1,2,0:T(8,128)(2,1)}), bf16[32,128,64]{1,2,0:T(8,128)(2,1)S(1)}, u32[]{:S(2)}, u32[]{:S(2)}) async-start(bf16[32,128,64]{1,2,0:T(8,128)(2,1)} %stack.7), calls=%async_computation | async-start | bytes 1048576 | tf_op jit(solution)/shard_map/while/body/eval_jaxpr/all_to_all | solution.py:119
  831.3 38.7 %all-to-all-start = ((bf16[32,128,64]{1,2,0:T(8,128)(2,1)}), bf16[32,128,64]{1,2,0:T(8,128)(2,1)S(1)}, u32[]{:S(2)}, u32[]{:S(2)}) async-start(bf16[32,128,64]{1,2,0:T(8,128)(2,1)} %stack.7), calls=%async_computation | async-start | bytes 1048576 | tf_op jit(solution)/shard_map/while/body/eval_jaxpr/all_to_all | solution.py:119
  881.3 38.7 %all-to-all-start = ((bf16[32,128,64]{1,2,0:T(8,128)(2,1)}), bf16[32,128,64]{1,2,0:T(8,128)(2,1)S(1)}, u32[]{:S(2)}, u32[]{:S(2)}) async-start(bf16[32,128,64]{1,2,0:T(8,128)(2,1)} %stack.7), calls=%async_computation | async-start | bytes 1048576 | tf_op jit(solution)/shard_map/while/body/eval_jaxpr/all_to_all | solution.py:119
  931.2 38.7 %all-to-all-start = ((bf16[32,128,64]{1,2,0:T(8,128)(2,1)}), bf16[32,128,64]{1,2,0:T(8,128)(2,1)S(1)}, u32[]{:S(2)}, u32[]{:S(2)}) async-start(bf16[32,128,64]{1,2,0:T(8,128)(2,1)} %stack.7), calls=%async_computation | async-start | bytes 1048576 | tf_op jit(solution)/shard_map/while/body/eval_jaxpr/all_to_all | solution.py:119
  981.1 38.7 %all-to-all-start = ((bf16[32,128,64]{1,2,0:T(8,128)(2,1)}), bf16[32,128,64]{1,2,0:T(8,128)(2,1)S(1)}, u32[]{:S(2)}, u32[]{:S(2)}) async-start(bf16[32,128,64]{1,2,0:T(8,128)(2,1)} %stack.7), calls=%async_computation | async-start | bytes 1048576 | tf_op jit(solution)/shard_map/while/body/eval_jaxpr/all_to_all | solution.py:119
  1031.0 38.7 %all-to-all-start = ((bf16[32,128,64]{1,2,0:T(8,128)(2,1)}), bf16[32,128,64]{1,2,0:T(8,128)(2,1)S(1)}, u32[]{:S(2)}, u32[]{:S(2)}) async-start(bf16[32,128,64]{1,2,0:T(8,128)(2,1)} %stack.7), calls=%async_computation | async-start | bytes 1048576 | tf_op jit(solution)/shard_map/while/body/eval_jaxpr/all_to_all | solution.py:119
  1080.9 38.7 %all-to-all-start = ((bf16[32,128,64]{1,2,0:T(8,128)(2,1)}), bf16[32,128,64]{1,2,0:T(8,128)(2,1)S(1)}, u32[]{:S(2)}, u32[]{:S(2)}) async-start(bf16[32,128,64]{1,2,0:T(8,128)(2,1)} %stack.7), calls=%async_computation | async-start | bytes 1048576 | tf_op jit(solution)/shard_map/while/body/eval_jaxpr/all_to_all | solution.py:119
  1130.9 38.7 %all-to-all-start = ((bf16[32,128,64]{1,2,0:T(8,128)(2,1)}), bf16[32,128,64]{1,2,0:T(8,128)(2,1)S(1)}, u32[]{:S(2)}, u32[]{:S(2)}) async-start(bf16[32,128,64]{1,2,0:T(8,128)(2,1)} %stack.7), calls=%async_computation | async-start | bytes 1048576 | tf_op jit(solution)/shard_map/while/body/eval_jaxpr/all_to_all | solution.py:119
  (28 other events, 237.8 us)
Sparse Core Ops, SparseCore 0:
  1180.6 68.0 all-gather.2
